TPU v7x, 128 devices: a whole 4x4x4 slice. The times are simulated.
128 devices in a mesh: rep: 16 (over z, x), fs: 4 (over y), tp: 2 (over core).
Axes of the slice: x: 4, y: 4, z: 4, core: 2. Of those that a mesh axis runs over, the one named last changes fastest.
Arguments:
- inputs: bfloat16 [16384, 2048], P(('rep', 'fs', 'tp')), may hold values from -6 to 6
- out_grad: bfloat16 [16384, 2048], P(('rep', 'fs', 'tp')), may hold values from -24 to 24
- pre_act: bfloat16 [16384, 8192], P('rep', ('fs', 'tp')), may hold values from -6 to 6
- w_up: bfloat16 [2048, 8192], P('rep', ('fs', 'tp')), may hold values from -0.125 to 0.125
- w_down_t: bfloat16 [2048, 8192], P('rep', ('fs', 'tp')), may hold values from -0.0625 to 0.0625
Outputs:
- grad_in: bfloat16 [16384, 2048], P(('rep', 'fs', 'tp'))
- grad_up: float32 [2048, 8192], P('rep', ('fs', 'tp'))
- grad_down_t: float32 [2048, 8192], P('rep', ('fs', 'tp'))
All inputs are finite; a program needn't handle non-finite values.
Results may differ from a plain program's by a relative error of at most 0.014.
Values may be sent and summed in bfloat16 or wider, within the bound.
A program may use at most 128 MiB of HBM per device.

v0:
```python
import jax
import jax.numpy as jnp
from jax import lax
from jax.sharding import PartitionSpec as P


def side_by_side(arrays, axis, dim, along):
    widths = [a.shape[along] for a in arrays]
    both = jnp.concatenate(arrays, axis=along)
    out = lax.all_gather(both, axis, axis=dim, tiled=True)
    return tuple(jnp.split(out, [sum(widths[:k]) for k in range(1, len(widths))], axis=along))


def cut_along(shard, dim, length):
    shape = shard.shape
    tiles = shard.reshape(*shape[:dim], length, shape[dim] // length, *shape[dim + 1 :])
    return jnp.moveaxis(tiles, dim, 0)


def sent_and_summed(shard, axis, dim):
    tiles = cut_along(shard, dim, lax.axis_size(axis))
    arrived = lax.all_to_all(tiles, axis, split_axis=0, concat_axis=0, tiled=True)
    return arrived.astype(jnp.float32).sum(axis=0)


def on_device(inputs, out_grad, pre_act, w_up, w_down_t):
    input_rows, grad_rows = side_by_side((inputs, out_grad), ("fs", "tp"), 0, 1)
    row_count, col_count = pre_act.shape
    pre_float = pre_act.astype(jnp.float32)
    linear = jnp.maximum(pre_float, 0.0)
    squared = (linear * linear).astype(jnp.bfloat16)
    grad_squared = jnp.dot(
        grad_rows,
        lax.all_gather(w_down_t, "rep", axis=0, tiled=True),
        preferred_element_type=jnp.float32,
    )
    grad_pre = (grad_squared * 2.0 * linear).astype(jnp.bfloat16)
    partial_terms = lax.dot_general(
        grad_pre,
        lax.all_gather(w_up, "rep", axis=0, tiled=True),
        (((1,), (1,)), ((), ())),
        preferred_element_type=jnp.float32,
    ).astype(jnp.bfloat16)
    grad_in = sent_and_summed(
        partial_terms.astype(jnp.float32).astype(jnp.bfloat16), ("fs", "tp"), 0
    ).astype(jnp.bfloat16)
    total_tokens = row_count * lax.axis_size("rep")
    factor = float(total_tokens) ** (-0.5)
    down_part = lax.dot_general(
        grad_rows, squared, (((0,), (0,)), ((), ())), preferred_element_type=jnp.float32
    )
    up_part = lax.dot_general(
        input_rows, grad_pre, (((0,), (0,)), ((), ())), preferred_element_type=jnp.float32
    )
    stacked = lax.psum_scatter(
        (jnp.concatenate([down_part, up_part], axis=1) * factor).astype(jnp.bfloat16),
        "rep",
        scatter_dimension=0,
        tiled=True,
    ).astype(jnp.float32)
    grad_down_t = stacked[:, :col_count]
    grad_up = stacked[:, col_count:]
    return (grad_in, grad_up, grad_down_t)


def solution(mesh):
    in_specs = (
        P(("rep", "fs", "tp"), None),
        P(("rep", "fs", "tp"), None),
        P("rep", ("fs", "tp")),
        P("rep", ("fs", "tp")),
        P("rep", ("fs", "tp")),
    )
    out_specs = (P(("rep", "fs", "tp"), None), P("rep", ("fs", "tp")), P("rep", ("fs", "tp")))
    return jax.shard_map(
        on_device, mesh=mesh, in_specs=in_specs, out_specs=out_specs, check_vma=False
    )
```

profile of v0, /device:TPU:0, one launch (start us, length us, event | category | flops | bytes accessed | tf_op | source)
XLA Modules:
  0.0 267.7 jit_solution(14350902395174839867)
XLA Ops:
  7.2 0.0 all-gather.4.cloned.1.call-start
  7.2 2.4 pad_maximum_fusion
  9.6 0.0 all-gather.4.cloned.1.call-update
  9.6 0.0 all-gather.6.cloned.1.call-start
  9.6 0.7 all-gather.6.cloned.1.call-update
  10.3 0.0 all-gather.8.cloned.1.call-start
  10.4 0.7 all-gather.8.cloned.1.call-update
  11.1 0.0 copy-start.1
  11.1 0.0 reduce-scatter.4.cloned.1.call-start
  11.1 50.8 %all-gather.4.cloned.1.call-done = bf16[1024,4096]{1,0:T(8,128)(2,1)} async-done(((bf16[128,4096]{1,0:T(8,128)(2,1)}), bf16[1024,4096]{1,0:T(8,128)(2,1)}) %all-gather.4.cloned.1.call-update) | async-done | bytes 8388624 | tf_op jit(solution)/shard_map/all_gather | solution.py:10
  61.9 10.7 %fusion.3 = f32[2048,1024]{0,1:T(8,128)} fusion(bf16[1024,4096]{1,0:T(8,128)(2,1)} %all-gather.4.cloned.1.call-done, bf16[1024,1024]{1,0:T(8,128)(2,1)} %param.7), kind=kOutput, calls=%fused_computation.8 | convolution fusion | flops 4299161600 | bytes 14680064 | tf_op jit(solution)/shard_map/dot_general | solution.py:49
  72.6 43.1 %all-gather.6.cloned.1.call-done = bf16[2048,1024]{1,0:T(8,128)(2,1)} async-done(((bf16[128,1024]{1,0:T(8,128)(2,1)}), bf16[2048,1024]{1,0:T(8,128)(2,1)}) %all-gather.6.cloned.1.call-update) | async-done | bytes 4194320 | tf_op jit(solution)/shard_map/all_gather | solution.py:34
  115.7 0.0 copy-done.1
  115.7 0.0 copy-start
  115.7 0.0 slice-start
  115.7 8.1 %multiply_convert_fusion.1 = bf16[1024,1024]{1,0:T(8,128)(2,1)S(1)} fusion(bf16[1024,1024]{1,0:T(8,128)(2,1)S(1)} %copy-done.1, bf16[2048,1024]{1,0:T(8,128)(2,1)} %all-gather.6.cloned.1.call-done, bf16[1024,4096]{1,0:T(8,128)(2,1)} %all-gather.4.cloned.1.call-done), kind=kOutput, calls=%fused_computation.5 | convolution fusion | flops 4300210176 | bytes 12582912 | tf_op jit(solution)/shard_map/dot_general | solution.py:32
  123.8 0.0 copy-done
  123.8 0.0 copy-start.2
  123.8 0.0 slice-start.1
  123.9 4.9 %fusion.1 = f32[2048,1024]{0,1:T(8,128)S(1)} fusion(bf16[1024,1024]{1,0:T(8,128)(2,1)S(1)} %multiply_convert_fusion.1, bf16[1024,4096]{1,0:T(8,128)(2,1)S(1)} %copy-done), kind=kOutput, calls=%fused_computation.2 | convolution fusion | flops 4294967296 | bytes 14680064 | tf_op jit(solution)/shard_map/dot_general | solution.py:52
  128.8 0.0 copy-done.2
  128.8 0.0 slice-done
  128.8 0.0 slice-done.1
  128.8 4.8 %fusion = bf16[2048,2048]{0,1:T(8,128)(2,1)} fusion(f32[2048,1024]{0,1:T(8,128)S(1)} %fusion.1, f32[2048,1024]{0,1:T(8,128)S(1)} %bitcast.7), kind=kLoop, calls=%fused_computation.1 | loop fusion | flops 12582912 | bytes 25165824 | tf_op jit(solution)/shard_map/convert_element_type | solution.py:56
  133.6 12.4 %copy.12 = bf16[2048,2048]{1,0:T(8,128)(2,1)} copy(bf16[2048,2048]{0,1:T(8,128)(2,1)} %fusion) | data formatting | bytes 16777216
  146.0 0.0 copy-start.3
  146.0 0.0 reduce-scatter.4.cloned.1.call-update
  146.0 22.9 %all-gather.8.cloned.1.call-done = bf16[2048,1024]{1,0:T(8,128)(2,1)} async-done(((bf16[128,1024]{1,0:T(8,128)(2,1)}), bf16[2048,1024]{1,0:T(8,128)(2,1)}) %all-gather.8.cloned.1.call-update) | async-done | bytes 4194320 | tf_op jit(solution)/shard_map/all_gather | solution.py:40
  169.0 0.0 copy-done.3
  169.0 6.9 %convolution_convert_fusion = bf16[1024,2048]{1,0:T(8,128)(2,1)S(1)} fusion(bf16[1024,1024]{1,0:T(8,128)(2,1)S(1)} %copy-done.3, bf16[2048,1024]{1,0:T(8,128)(2,1)} %all-gather.8.cloned.1.call-done), kind=kOutput, calls=%fused_computation.7 | convolution fusion | flops 4297064448 | bytes 10485760 | tf_op jit(solution)/shard_map/dot_general | solution.py:38
  175.9 53.9 %all_to_all.5 = bf16[8,128,2048]{2,1,0:T(8,128)(2,1)} all-to-all(bf16[8,128,2048]{2,1,0:T(8,128)(2,1)S(1)} %bitcast.8), channel_id=1, replica_groups=mesh['rep'=16,'fs'=4,'tp'=2] {'fs','tp'}, dimensions={0} | all-to-all | bytes 8388608 | tf_op jit(solution)/shard_map/all_to_all | solution.py:22
  229.8 3.9 %reduce_sum.12 = bf16[128,2048]{1,0:T(8,128)(2,1)} reduce(bf16[8,128,2048]{2,1,0:T(8,128)(2,1)} %all_to_all.5, bf16[]{:T(256)} %constant.3.clone.1), dimensions={0}, to_apply=%region_0.0 | reduce | flops 1835008 | bytes 4718594 | tf_op jit(solution)/shard_map/reduce_sum | solution.py:23
  233.6 24.1 %reduce-scatter.4.cloned.1.call-done = bf16[128,2048]{1,0:T(8,128)(2,1)} async-done(((bf16[2048,2048]{1,0:T(8,128)(2,1)}), bf16[128,2048]{1,0:T(8,128)(2,1)}) %reduce-scatter.4.cloned.1.call-update) | async-done | bytes 524304
  257.8 1.3 copy.13
  259.1 0.1 fusion.11
  259.2 1.0 copy.11
  260.2 1.0 copy.10
  (1 shorter events, 0.0 us)
Async XLA Ops:
  7.2 54.7 %all-gather.4.cloned.1.call-start = ((), (), s32[]{:S(2)}) async-start(), calls=%async_computation.2 | async-start | bytes 9437184 | tf_op jit(solution)/shard_map/all_gather | solution.py:10
  9.6 106.1 %all-gather.6.cloned.1.call-start = ((), (), s32[]{:S(2)}) async-start(), calls=%async_computation.3 | async-start | bytes 4456448 | tf_op jit(solution)/shard_map/all_gather | solution.py:34
  10.3 158.6 %all-gather.8.cloned.1.call-start = ((), (), s32[]{:S(2)}) async-start(), calls=%async_computation.4 | async-start | bytes 4456448 | tf_op jit(solution)/shard_map/all_gather | solution.py:40
  11.1 104.6 %copy-start.1 = (bf16[1024,1024]{1,0:T(8,128)(2,1)S(1)}, bf16[1024,1024]{1,0:T(8,128)(2,1)}, u32[]{:S(2)}) copy-start(bf16[1024,1024]{1,0:T(8,128)(2,1)} %param.7) | copy-start | bytes 6291460
  11.1 246.7 %reduce-scatter.4.cloned.1.call-start = ((), (), s32[]{:S(2)}) async-start(), calls=%async_computation.5 | async-start | bytes 8912896
  115.7 8.1 %copy-start = (bf16[1024,4096]{1,0:T(8,128)(2,1)S(1)}, bf16[1024,4096]{1,0:T(8,128)(2,1)}, u32[]{:S(2)}) copy-start(bf16[1024,4096]{1,0:T(8,128)(2,1)} %all-gather.4.cloned.1.call-done) | copy-start | bytes 25165828
  115.7 13.1 %slice-start = ((s8[8388608]{0:T(1024)(128)(4,1)}), s8[4194304]{0:T(1024)(128)(4,1)S(1)}, s32[]{:S(2)}) async-start(s8[8388608]{0:T(1024)(128)(4,1)} %bitcast.6), calls=%async_computation.6 | async-start | bytes 8388608
  123.8 5.0 %copy-start.2 = (bf16[1024,1024]{1,0:T(8,128)(2,1)}, bf16[1024,1024]{1,0:T(8,128)(2,1)S(1)}, u32[]{:S(2)}) copy-start(bf16[1024,1024]{1,0:T(8,128)(2,1)S(1)} %multiply_convert_fusion.1) | copy-start | bytes 6291460
  123.8 5.0 %slice-start.1 = ((s8[8388608]{0:T(1024)(128)(4,1)}), s8[4194304]{0:T(1024)(128)(4,1)S(1)}, s32[]{:S(2)}) async-start(s8[8388608]{0:T(1024)(128)(4,1)} %bitcast.6), calls=%async_computation.7 | async-start | bytes 8388608
  146.0 23.0 %copy-start.3 = (bf16[1024,1024]{1,0:T(8,128)(2,1)S(1)}, bf16[1024,1024]{1,0:T(8,128)(2,1)}, u32[]{:S(2)}) copy-start(bf16[1024,1024]{1,0:T(8,128)(2,1)} %copy-done.2) | copy-start | bytes 6291460
Sparse Core Ops, SparseCore 0:
  9.7 52.1 all-gather.3
  64.0 51.6 all-gather.5
  117.9 51.0 all-gather.7
  172.2 85.5 reduce-scatter.3
where the time goes:
time: 268 us
  waiting for transfers between devices  142 us (53%)
  blocking collectives  53.9 us (20%)
  matrix products  30.7 us (11%)
  local copies, waits for them, and re-layouts  15.8 us (6%)
  between operations  13.9 us (5%)
  other arithmetic  11 us (4%)
    all_to_all x1, blocking collectives, sent_and_summed(): lax.all_to_all(tiles, axis, split_axis=0, concat_axis=0, tiled=True)  53.9 us
    all_gather x1, waiting for transfers between devices, side_by_side(): out = lax.all_gather(both, axis, axis=dim, tiled=True)  50.8 us
    all_gather x1, waiting for transfers between devices, on_device(): lax.all_gather(w_down_t, 'rep', axis=0, tiled=True)  43.1 us
    unnamed x5, waiting for transfers between devices  25.6 us
    all_gather x1, waiting for transfers between devices, on_device(): lax.all_gather(w_up, 'rep', axis=0, tiled=True)  22.9 us
    unnamed x16, local copies, waits for them, and re-layouts  15.7 us
    dot_general x1, matrix products, on_device(): lax.dot_general(grad_rows, squared, (((0,), (0,)), ((), ())), preferred_e...  10.7 us
    dot_general x1, matrix products, on_device(): jnp.dot(grad_rows, lax.all_gather(w_down_t, 'rep', axis=0, tiled=True), p...  8.1 us
  transfers between devices with their start and end apart: 4, of which 4 were waited for; matrix products, arithmetic and copies ran while one was open for 19% of the time, Pallas kernels for 0%

commit v1 on v0

--- a/solution.py
+++ b/solution.py
@@ -2,6 +2,24 @@
 import jax.numpy as jnp
 from jax import lax
 from jax.sharding import PartitionSpec as P
+
+
+def gather_around(array, axis, dim):
+    ways, here, step = (lax.axis_size(axis), lax.axis_index(axis), array.shape[dim])
+    shape = [n * ways if d == dim else n for d, n in enumerate(array.shape)]
+    full = lax.dynamic_update_slice_in_dim(
+        jnp.zeros(shape, array.dtype), array, here * step, axis=dim
+    )
+    going_up = going_down = array
+    for far in range(1, ways // 2 + 1):
+        going_up = lax.ppermute(going_up, axis, [(d, (d + 1) % ways) for d in range(ways)])
+        full = lax.dynamic_update_slice_in_dim(full, going_up, (here - far) % ways * step, axis=dim)
+        if 2 * far < ways:
+            going_down = lax.ppermute(going_down, axis, [(d, (d - 1) % ways) for d in range(ways)])
+            full = lax.dynamic_update_slice_in_dim(
+                full, going_down, (here + far) % ways * step, axis=dim
+            )
+    return full
 
 
 def side_by_side(arrays, axis, dim, along):
@@ -37,7 +55,7 @@
     grad_pre = (grad_squared * 2.0 * linear).astype(jnp.bfloat16)
     partial_terms = lax.dot_general(
         grad_pre,
-        lax.all_gather(w_up, "rep", axis=0, tiled=True),
+        gather_around(w_up, "rep", 0),
         (((1,), (1,)), ((), ())),
         preferred_element_type=jnp.float32,
     ).astype(jnp.bfloat16)

time: 268 us -> 332 us (1.24)
  starting transfers between devices: 0.16 us -> 39.3 us
  local copies, waits for them, and re-layouts: 15.8 us -> 30.8 us
  waiting for transfers between devices: 142 us -> 148 us
    ppermute x0 -> x15, waiting for transfers between devices: none -> 52.3 us  [the longest x8 41.8 us: gather_around(): lax.ppermute(going_up, axis, [(d, (d + 1) % ways) for d in range(ways)])]
    ppermute x0 -> x15, starting transfers between devices: none -> 39.2 us  [the longest x7 37.7 us: gather_around(): lax.ppermute(going_down, axis, [(d, (d - 1) % ways) for d in range(ways)])]
    unnamed x5 -> x4, waiting for transfers between devices: 25.6 us -> 0.73 us
    all_gather x1 -> x0, waiting for transfers between devices: 22.9 us -> none  [on_device(): lax.all_gather(w_up, 'rep', axis=0, tiled=True)]
    dynamic_update_slice x0 -> x16, local copies, waits for them, and re-layouts: none -> 11.6 us  [the longest x8 5.76 us: gather_around(): lax.dynamic_update_slice_in_dim(full, going_up, (here - far) % ways * ste...]
  transfers between devices with their start and end apart: 4 -> 18, of which waited for: 4 -> 14; matrix products, arithmetic and copies ran while one was open for 19% -> 11% of each run, Pallas kernels for 0% -> 0%
where the time goes in v1:
time: 332 us; the launch traced here: 331 us
  waiting for transfers between devices  148 us (45%)
  blocking collectives  56.7 us (17%)
  starting transfers between devices  39.3 us (12%)
  matrix products  31.3 us (9%)
  local copies, waits for them, and re-layouts  30.8 us (9%)
  between operations  13.9 us (4%)
  other arithmetic  11 us (3%)
    all_to_all x1, blocking collectives, sent_and_summed(): lax.all_to_all(tiles, axis, split_axis=0, concat_axis=0, tiled=True)  56.7 us
    all_gather x1, waiting for transfers between devices, side_by_side(): out = lax.all_gather(both, axis, axis=dim, tiled=True)  51.5 us
    all_gather x1, waiting for transfers between devices, on_device(): lax.all_gather(w_down_t, 'rep', axis=0, tiled=True)  43.2 us
    ppermute x8, waiting for transfers between devices, gather_around(): lax.ppermute(going_up, axis, [(d, (d + 1) % ways) for d in range(ways)])  41.8 us
    ppermute x7, starting transfers between devices, gather_around(): lax.ppermute(going_down, axis, [(d, (d - 1) % ways) for d in range(ways)])  37.7 us
    unnamed x16, local copies, waits for them, and re-layouts  16.6 us
    dot_general x1, matrix products, on_device(): lax.dot_general(grad_rows, squared, (((0,), (0,)), ((), ())), preferred_e...  10.6 us
    ppermute x7, waiting for transfers between devices, gather_around(): lax.ppermute(going_down, axis, [(d, (d - 1) % ways) for d in range(ways)])  10.5 us
  transfers between devices with their start and end apart: 18, of which 14 were waited for; matrix products, arithmetic and copies ran while one was open for 11% of the time, Pallas kernels for 0%

profile of v1, /device:TPU:0, one launch (start us, length us, event | category | flops | bytes accessed | tf_op | source)
XLA Modules:
  0.0 330.6 jit_solution(11238803849485627972)
XLA Ops:
  7.2 0.0 all-gather.3.cloned.1.call-start
  7.2 2.4 pad_maximum_fusion
  9.6 0.0 all-gather.3.cloned.1.call-update
  9.6 0.0 all-gather.5.cloned.1.call-start
  9.6 0.7 all-gather.5.cloned.1.call-update
  10.4 0.0 reduce-scatter.4.cloned.1.call-start
  10.4 51.5 %all-gather.3.cloned.1.call-done = bf16[1024,4096]{1,0:T(8,128)(2,1)} async-done(((bf16[128,4096]{1,0:T(8,128)(2,1)}), bf16[1024,4096]{1,0:T(8,128)(2,1)}) %all-gather.3.cloned.1.call-update) | async-done | bytes 8388624 | tf_op jit(solution)/shard_map/all_gather | solution.py:28
  61.9 10.6 %fusion.3 = f32[2048,1024]{0,1:T(8,128)} fusion(bf16[1024,4096]{1,0:T(8,128)(2,1)} %all-gather.3.cloned.1.call-done, bf16[1024,1024]{1,0:T(8,128)(2,1)} %param.7), kind=kOutput, calls=%fused_computation.8 | convolution fusion | flops 4299161600 | bytes 14680064 | tf_op jit(solution)/shard_map/dot_general | solution.py:67
  72.6 43.2 %all-gather.5.cloned.1.call-done = bf16[2048,1024]{1,0:T(8,128)(2,1)} async-done(((bf16[128,1024]{1,0:T(8,128)(2,1)}), bf16[2048,1024]{1,0:T(8,128)(2,1)}) %all-gather.5.cloned.1.call-update) | async-done | bytes 4194320 | tf_op jit(solution)/shard_map/all_gather | solution.py:52
  115.7 8.7 %multiply_convert_fusion.1 = bf16[1024,1024]{1,0:T(8,128)(2,1)S(1)} fusion(bf16[1024,1024]{1,0:T(8,128)(2,1)} %param.7, bf16[2048,1024]{1,0:T(8,128)(2,1)} %all-gather.5.cloned.1.call-done, bf16[1024,4096]{1,0:T(8,128)(2,1)} %all-gather.3.cloned.1.call-done), kind=kOutput, calls=%fused_computation.5 | convolution fusion | flops 4300210176 | bytes 12582912 | tf_op jit(solution)/shard_map/dot_general | solution.py:50
  124.5 4.9 %fusion.1 = f32[2048,1024]{0,1:T(8,128)S(1)} fusion(bf16[1024,1024]{1,0:T(8,128)(2,1)S(1)} %multiply_convert_fusion.1, bf16[1024,4096]{1,0:T(8,128)(2,1)S(1)} %copy-done.1), kind=kOutput, calls=%fused_computation.2 | convolution fusion | flops 4294967296 | bytes 14680064 | tf_op jit(solution)/shard_map/dot_general | solution.py:70
  129.5 4.8 %fusion = bf16[2048,2048]{0,1:T(8,128)(2,1)} fusion(f32[2048,1024]{0,1:T(8,128)S(1)} %fusion.1, f32[2048,1024]{0,1:T(8,128)S(1)} %bitcast.7), kind=kLoop, calls=%fused_computation.1 | loop fusion | flops 12582912 | bytes 25165824 | tf_op jit(solution)/shard_map/convert_element_type | solution.py:74
  134.2 12.4 %copy.12 = bf16[2048,2048]{1,0:T(8,128)(2,1)} copy(bf16[2048,2048]{0,1:T(8,128)(2,1)} %fusion) | data formatting | bytes 16777216
  146.6 0.0 reduce-scatter.4.cloned.1.call-update
  146.6 0.9 copy-done
  147.5 1.5 collective-permute-start
  149.0 3.9 %collective-permute-start.1 = (bf16[128,1024]{1,0:T(8,128)(2,1)S(1)}, bf16[128,1024]{1,0:T(8,128)(2,1)S(1)}, u32[]{:S(2)}, u32[]{:S(2)}) collective-permute-start(bf16[128,1024]{1,0:T(8,128)(2,1)S(1)} %copy-done), channel_id=1, source_target_pairs={{0,120},{8,0},{16,8},{24,16},{32,24},{40,32},{48,40},{56,48},{64,5... | collective-permute-start | bytes 786440 | tf_op jit(solution)/shard_map/ppermute | solution.py:18
  152.9 5.9 %collective-permute-done = bf16[128,1024]{1,0:T(8,128)(2,1)S(1)} collective-permute-done((bf16[128,1024]{1,0:T(8,128)(2,1)S(1)}, bf16[128,1024]{1,0:T(8,128)(2,1)S(1)}, u32[]{:S(2)}, u32[]{:S(2)}) %collective-permute-start) | collective-permute-done | bytes 262176 | tf_op jit(solution)/shard_map/ppermute | solution.py:15
  158.7 0.0 collective-permute-start.2
  158.7 2.8 collective-permute-done.1
  161.6 5.8 %collective-permute-start.3 = (bf16[128,1024]{1,0:T(8,128)(2,1)S(1)}, bf16[128,1024]{1,0:T(8,128)(2,1)S(1)}, u32[]{:S(2)}, u32[]{:S(2)}) collective-permute-start(bf16[128,1024]{1,0:T(8,128)(2,1)S(1)} %collective-permute-done.1), channel_id=1, source_target_pairs={{0,120},{8,0},{16,8},{24,16},{32,24},{40,32},{48,40},{56,48},{64,5... | collective-permute-start | bytes 786440 | tf_op jit(solution)/shard_map/ppermute | solution.py:18
  167.4 7.9 %collective-permute-done.2 = bf16[128,1024]{1,0:T(8,128)(2,1)S(1)} collective-permute-done((bf16[128,1024]{1,0:T(8,128)(2,1)S(1)}, bf16[128,1024]{1,0:T(8,128)(2,1)S(1)}, u32[]{:S(2)}, u32[]{:S(2)}) %collective-permute-start.2) | collective-permute-done | bytes 262176 | tf_op jit(solution)/shard_map/ppermute | solution.py:15
  175.3 0.0 collective-permute-done.3
  175.3 5.3 %collective-permute-start.5 = (bf16[128,1024]{1,0:T(8,128)(2,1)S(1)}, bf16[128,1024]{1,0:T(8,128)(2,1)S(1)}, u32[]{:S(2)}, u32[]{:S(2)}) collective-permute-start(bf16[128,1024]{1,0:T(8,128)(2,1)S(1)} %collective-permute-done.3), channel_id=1, source_target_pairs={{0,120},{8,0},{16,8},{24,16},{32,24},{40,32},{48,40},{56,48},{64,5... | collective-permute-start | bytes 786440 | tf_op jit(solution)/shard_map/ppermute | solution.py:18
  180.7 10.0 %collective-permute-done.4 = bf16[128,1024]{1,0:T(8,128)(2,1)S(1)} collective-permute-done((bf16[128,1024]{1,0:T(8,128)(2,1)S(1)}, bf16[128,1024]{1,0:T(8,128)(2,1)S(1)}, u32[]{:S(2)}, u32[]{:S(2)}) %collective-permute-start.4) | collective-permute-done | bytes 262176 | tf_op jit(solution)/shard_map/ppermute | solution.py:15
  190.7 2.5 broadcast_in_dim.3
  193.2 0.7 constant_dynamic-update-slice_fusion.15
  193.9 0.7 constant_dynamic-update-slice_fusion.14
  194.6 0.0 collective-permute-done.5
  194.6 5.3 %collective-permute-start.7 = (bf16[128,1024]{1,0:T(8,128)(2,1)S(1)}, bf16[128,1024]{1,0:T(8,128)(2,1)S(1)}, u32[]{:S(2)}, u32[]{:S(2)}) collective-permute-start(bf16[128,1024]{1,0:T(8,128)(2,1)S(1)} %collective-permute-done.5), channel_id=1, source_target_pairs={{0,120},{8,0},{16,8},{24,16},{32,24},{40,32},{48,40},{56,48},{64,5... | collective-permute-start | bytes 786440 | tf_op jit(solution)/shard_map/ppermute | solution.py:18
  200.0 0.7 constant_dynamic-update-slice_fusion.13
  200.7 5.2 %collective-permute-done.6 = bf16[128,1024]{1,0:T(8,128)(2,1)S(1)} collective-permute-done((bf16[128,1024]{1,0:T(8,128)(2,1)S(1)}, bf16[128,1024]{1,0:T(8,128)(2,1)S(1)}, u32[]{:S(2)}, u32[]{:S(2)}) %collective-permute-start.6) | collective-permute-done | bytes 262176 | tf_op jit(solution)/shard_map/ppermute | solution.py:15
  205.9 0.7 constant_dynamic-update-slice_fusion.12
  206.7 0.7 constant_dynamic-update-slice_fusion.11
  207.4 1.5 collective-permute-done.7
  208.9 5.8 %collective-permute-start.9 = (bf16[128,1024]{1,0:T(8,128)(2,1)S(1)}, bf16[128,1024]{1,0:T(8,128)(2,1)S(1)}, u32[]{:S(2)}, u32[]{:S(2)}) collective-permute-start(bf16[128,1024]{1,0:T(8,128)(2,1)S(1)} %collective-permute-done.7), channel_id=1, source_target_pairs={{0,120},{8,0},{16,8},{24,16},{32,24},{40,32},{48,40},{56,48},{64,5... | collective-permute-start | bytes 786440 | tf_op jit(solution)/shard_map/ppermute | solution.py:18
  214.7 0.7 constant_dynamic-update-slice_fusion.10
  215.4 1.8 collective-permute-done.8
  217.2 0.0 collective-permute-start.10
  217.2 0.7 constant_dynamic-update-slice_fusion.9
  218.0 0.7 constant_dynamic-update-slice_fusion.8
  218.7 5.7 %collective-permute-start.11 = (bf16[128,1024]{1,0:T(8,128)(2,1)S(1)}, bf16[128,1024]{1,0:T(8,128)(2,1)S(1)}, u32[]{:S(2)}, u32[]{:S(2)}) collective-permute-start(bf16[128,1024]{1,0:T(8,128)(2,1)S(1)} %collective-permute-done.9), channel_id=1, source_target_pairs={{0,120},{8,0},{16,8},{24,16},{32,24},{40,32},{48,40},{56,48},{64,5... | collective-permute-start | bytes 786440 | tf_op jit(solution)/shard_map/ppermute | solution.py:18
  224.4 0.7 constant_dynamic-update-slice_fusion.7
  225.1 1.8 collective-permute-done.10
  226.9 0.0 collective-permute-start.12
  226.9 0.7 constant_dynamic-update-slice_fusion.6
  227.6 0.7 constant_dynamic-update-slice_fusion.5
  228.4 5.9 %collective-permute-done.11 = bf16[128,1024]{1,0:T(8,128)(2,1)S(1)} collective-permute-done((bf16[128,1024]{1,0:T(8,128)(2,1)S(1)}, bf16[128,1024]{1,0:T(8,128)(2,1)S(1)}, u32[]{:S(2)}, u32[]{:S(2)}) %collective-permute-start.11) | collective-permute-done | bytes 262176 | tf_op jit(solution)/shard_map/ppermute | solution.py:18
  234.3 5.8 %collective-permute-start.13 = (bf16[128,1024]{1,0:T(8,128)(2,1)S(1)}, bf16[128,1024]{1,0:T(8,128)(2,1)S(1)}, u32[]{:S(2)}, u32[]{:S(2)}) collective-permute-start(bf16[128,1024]{1,0:T(8,128)(2,1)S(1)} %collective-permute-done.11), channel_id=1, source_target_pairs={{0,120},{8,0},{16,8},{24,16},{32,24},{40,32},{48,40},{56,48},{64,5... | collective-permute-start | bytes 786440 | tf_op jit(solution)/shard_map/ppermute | solution.py:18
  240.1 0.7 constant_dynamic-update-slice_fusion.4
  240.8 1.9 collective-permute-done.12
  242.7 0.7 constant_dynamic-update-slice_fusion.3
  243.4 0.7 constant_dynamic-update-slice_fusion.2
  244.1 0.2 collective-permute-done.13
  244.4 0.7 constant_dynamic-update-slice_fusion.1
  245.1 7.3 %collective-permute-done.14 = bf16[128,1024]{1,0:T(8,128)(2,1)S(1)} collective-permute-done((bf16[128,1024]{1,0:T(8,128)(2,1)S(1)}, bf16[128,1024]{1,0:T(8,128)(2,1)S(1)}, u32[]{:S(2)}, u32[]{:S(2)}) %collective-permute-start.14) | collective-permute-done | bytes 262176 | tf_op jit(solution)/shard_map/ppermute | solution.py:15
  252.4 0.7 constant_dynamic-update-slice_fusion
  253.1 7.0 %convolution_convert_fusion = bf16[1024,2048]{1,0:T(8,128)(2,1)S(1)} fusion(bf16[1024,1024]{1,0:T(8,128)(2,1)S(1)} %copy-done.3, bf16[2048,1024]{1,0:T(8,128)(2,1)} %constant_dynamic-update-slice_fusion), kind=kOutput, calls=%fused_computation.7 | convolution fusion | flops 4297064448 | bytes 10485760 | tf_op jit(solution)/shard_map/dot_general | solution.py:56
  260.2 56.7 %all_to_all.5 = bf16[8,128,2048]{2,1,0:T(8,128)(2,1)} all-to-all(bf16[8,128,2048]{2,1,0:T(8,128)(2,1)S(1)} %bitcast.8), channel_id=1, replica_groups=mesh['rep'=16,'fs'=4,'tp'=2] {'fs','tp'}, dimensions={0} | all-to-all | bytes 8388608 | tf_op jit(solution)/shard_map/all_to_all | solution.py:40
  316.9 3.8 %reduce_sum.12 = bf16[128,2048]{1,0:T(8,128)(2,1)} reduce(bf16[8,128,2048]{2,1,0:T(8,128)(2,1)} %all_to_all.5, bf16[]{:T(256)} %constant.97.clone.1), dimensions={0}, to_apply=%region_0.1 | reduce | flops 1835008 | bytes 4718594 | tf_op jit(solution)/shard_map/reduce_sum | solution.py:41
  320.7 1.3 copy.13
  322.0 0.1 fusion.11
  322.1 1.0 copy.11
  323.1 1.0 copy.10
  (18 shorter events, 0.0 us)
Async XLA Ops:
  7.2 54.7 %all-gather.3.cloned.1.call-start = ((), (), s32[]{:S(2)}) async-start(), calls=%async_computation.2 | async-start | bytes 9437184 | tf_op jit(solution)/shard_map/all_gather | solution.py:28
  9.6 106.1 %all-gather.5.cloned.1.call-start = ((), (), s32[]{:S(2)}) async-start(), calls=%async_computation.3 | async-start | bytes 4456448 | tf_op jit(solution)/shard_map/all_gather | solution.py:52
  10.4 310.4 %reduce-scatter.4.cloned.1.call-start = ((), (), s32[]{:S(2)}) async-start(), calls=%async_computation.4 | async-start | bytes 8912896
  115.7 8.7 %copy-start.1 = (bf16[1024,4096]{1,0:T(8,128)(2,1)S(1)}, bf16[1024,4096]{1,0:T(8,128)(2,1)}, u32[]{:S(2)}) copy-start(bf16[1024,4096]{1,0:T(8,128)(2,1)} %all-gather.3.cloned.1.call-done) | copy-start | bytes 25165828
  115.7 13.7 %slice-start = ((s8[8388608]{0:T(1024)(128)(4,1)}), s8[4194304]{0:T(1024)(128)(4,1)S(1)}, s32[]{:S(2)}) async-start(s8[8388608]{0:T(1024)(128)(4,1)} %bitcast.6), calls=%async_computation.5 | async-start | bytes 8388608
  124.4 5.0 %copy-start.2 = (bf16[1024,1024]{1,0:T(8,128)(2,1)}, bf16[1024,1024]{1,0:T(8,128)(2,1)S(1)}, u32[]{:S(2)}) copy-start(bf16[1024,1024]{1,0:T(8,128)(2,1)S(1)} %multiply_convert_fusion.1) | copy-start | bytes 6291460
  124.4 5.0 %slice-start.1 = ((s8[8388608]{0:T(1024)(128)(4,1)}), s8[4194304]{0:T(1024)(128)(4,1)S(1)}, s32[]{:S(2)}) async-start(s8[8388608]{0:T(1024)(128)(4,1)} %bitcast.6), calls=%async_computation.6 | async-start | bytes 8388608
  146.6 0.9 copy-start
  147.5 11.2 %collective-permute-start = (bf16[128,1024]{1,0:T(8,128)(2,1)S(1)}, bf16[128,1024]{1,0:T(8,128)(2,1)S(1)}, u32[]{:S(2)}, u32[]{:S(2)}) collective-permute-start(bf16[128,1024]{1,0:T(8,128)(2,1)S(1)} %copy-done), channel_id=1, source_target_pairs={{0,8},{8,16},{16,24},{24,32},{32,40},{40,48},{48,56},{56,64},{64,7... | collective-permute-start | bytes 786440 | tf_op jit(solution)/shard_map/ppermute | solution.py:15
  149.0 12.6 %collective-permute-start.1 = (bf16[128,1024]{1,0:T(8,128)(2,1)S(1)}, bf16[128,1024]{1,0:T(8,128)(2,1)S(1)}, u32[]{:S(2)}, u32[]{:S(2)}) collective-permute-start(bf16[128,1024]{1,0:T(8,128)(2,1)S(1)} %copy-done), channel_id=1, source_target_pairs={{0,120},{8,0},{16,8},{24,16},{32,24},{40,32},{48,40},{56,48},{64,5... | collective-permute-start | bytes 786440 | tf_op jit(solution)/shard_map/ppermute | solution.py:18
  158.7 16.6 %collective-permute-start.2 = (bf16[128,1024]{1,0:T(8,128)(2,1)S(1)}, bf16[128,1024]{1,0:T(8,128)(2,1)S(1)}, u32[]{:S(2)}, u32[]{:S(2)}) collective-permute-start(bf16[128,1024]{1,0:T(8,128)(2,1)S(1)} %collective-permute-done), channel_id=1, source_target_pairs={{0,8},{8,16},{16,24},{24,32},{32,40},{40,48},{48,56},{56,64},{64,7... | collective-permute-start | bytes 786440 | tf_op jit(solution)/shard_map/ppermute | solution.py:15
  161.6 13.7 %collective-permute-start.3 = (bf16[128,1024]{1,0:T(8,128)(2,1)S(1)}, bf16[128,1024]{1,0:T(8,128)(2,1)S(1)}, u32[]{:S(2)}, u32[]{:S(2)}) collective-permute-start(bf16[128,1024]{1,0:T(8,128)(2,1)S(1)} %collective-permute-done.1), channel_id=1, source_target_pairs={{0,120},{8,0},{16,8},{24,16},{32,24},{40,32},{48,40},{56,48},{64,5... | collective-permute-start | bytes 786440 | tf_op jit(solution)/shard_map/ppermute | solution.py:18
  175.3 15.3 %collective-permute-start.4 = (bf16[128,1024]{1,0:T(8,128)(2,1)S(1)}, bf16[128,1024]{1,0:T(8,128)(2,1)S(1)}, u32[]{:S(2)}, u32[]{:S(2)}) collective-permute-start(bf16[128,1024]{1,0:T(8,128)(2,1)S(1)} %collective-permute-done.2), channel_id=1, source_target_pairs={{0,8},{8,16},{16,24},{24,32},{32,40},{40,48},{48,56},{56,64},{64,7... | collective-permute-start | bytes 786440 | tf_op jit(solution)/shard_map/ppermute | solution.py:15
  175.3 19.3 %collective-permute-start.5 = (bf16[128,1024]{1,0:T(8,128)(2,1)S(1)}, bf16[128,1024]{1,0:T(8,128)(2,1)S(1)}, u32[]{:S(2)}, u32[]{:S(2)}) collective-permute-start(bf16[128,1024]{1,0:T(8,128)(2,1)S(1)} %collective-permute-done.3), channel_id=1, source_target_pairs={{0,120},{8,0},{16,8},{24,16},{32,24},{40,32},{48,40},{56,48},{64,5... | collective-permute-start | bytes 786440 | tf_op jit(solution)/shard_map/ppermute | solution.py:18
  190.7 15.3 %collective-permute-start.6 = (bf16[128,1024]{1,0:T(8,128)(2,1)S(1)}, bf16[128,1024]{1,0:T(8,128)(2,1)S(1)}, u32[]{:S(2)}, u32[]{:S(2)}) collective-permute-start(bf16[128,1024]{1,0:T(8,128)(2,1)S(1)} %collective-permute-done.4), channel_id=1, source_target_pairs={{0,8},{8,16},{16,24},{24,32},{32,40},{40,48},{48,56},{56,64},{64,7... | collective-permute-start | bytes 786440 | tf_op jit(solution)/shard_map/ppermute | solution.py:15
  193.9 59.2 %copy-start.3 = (bf16[1024,1024]{1,0:T(8,128)(2,1)S(1)}, bf16[1024,1024]{1,0:T(8,128)(2,1)}, u32[]{:S(2)}) copy-start(bf16[1024,1024]{1,0:T(8,128)(2,1)} %copy-done.2) | copy-start | bytes 6291460
  194.6 14.3 %collective-permute-start.7 = (bf16[128,1024]{1,0:T(8,128)(2,1)S(1)}, bf16[128,1024]{1,0:T(8,128)(2,1)S(1)}, u32[]{:S(2)}, u32[]{:S(2)}) collective-permute-start(bf16[128,1024]{1,0:T(8,128)(2,1)S(1)} %collective-permute-done.5), channel_id=1, source_target_pairs={{0,120},{8,0},{16,8},{24,16},{32,24},{40,32},{48,40},{56,48},{64,5... | collective-permute-start | bytes 786440 | tf_op jit(solution)/shard_map/ppermute | solution.py:18
  205.9 11.3 %collective-permute-start.8 = (bf16[128,1024]{1,0:T(8,128)(2,1)S(1)}, bf16[128,1024]{1,0:T(8,128)(2,1)S(1)}, u32[]{:S(2)}, u32[]{:S(2)}) collective-permute-start(bf16[128,1024]{1,0:T(8,128)(2,1)S(1)} %collective-permute-done.6), channel_id=1, source_target_pairs={{0,8},{8,16},{16,24},{24,32},{32,40},{40,48},{48,56},{56,64},{64,7... | collective-permute-start | bytes 786440 | tf_op jit(solution)/shard_map/ppermute | solution.py:15
  208.9 9.8 %collective-permute-start.9 = (bf16[128,1024]{1,0:T(8,128)(2,1)S(1)}, bf16[128,1024]{1,0:T(8,128)(2,1)S(1)}, u32[]{:S(2)}, u32[]{:S(2)}) collective-permute-start(bf16[128,1024]{1,0:T(8,128)(2,1)S(1)} %collective-permute-done.7), channel_id=1, source_target_pairs={{0,120},{8,0},{16,8},{24,16},{32,24},{40,32},{48,40},{56,48},{64,5... | collective-permute-start | bytes 786440 | tf_op jit(solution)/shard_map/ppermute | solution.py:18
  217.2 9.7 %collective-permute-start.10 = (bf16[128,1024]{1,0:T(8,128)(2,1)S(1)}, bf16[128,1024]{1,0:T(8,128)(2,1)S(1)}, u32[]{:S(2)}, u32[]{:S(2)}) collective-permute-start(bf16[128,1024]{1,0:T(8,128)(2,1)S(1)} %collective-permute-done.8), channel_id=1, source_target_pairs={{0,8},{8,16},{16,24},{24,32},{32,40},{40,48},{48,56},{56,64},{64,7... | collective-permute-start | bytes 786440 | tf_op jit(solution)/shard_map/ppermute | solution.py:15
  218.7 15.6 %collective-permute-start.11 = (bf16[128,1024]{1,0:T(8,128)(2,1)S(1)}, bf16[128,1024]{1,0:T(8,128)(2,1)S(1)}, u32[]{:S(2)}, u32[]{:S(2)}) collective-permute-start(bf16[128,1024]{1,0:T(8,128)(2,1)S(1)} %collective-permute-done.9), channel_id=1, source_target_pairs={{0,120},{8,0},{16,8},{24,16},{32,24},{40,32},{48,40},{56,48},{64,5... | collective-permute-start | bytes 786440 | tf_op jit(solution)/shard_map/ppermute | solution.py:18
  226.9 15.8 %collective-permute-start.12 = (bf16[128,1024]{1,0:T(8,128)(2,1)S(1)}, bf16[128,1024]{1,0:T(8,128)(2,1)S(1)}, u32[]{:S(2)}, u32[]{:S(2)}) collective-permute-start(bf16[128,1024]{1,0:T(8,128)(2,1)S(1)} %collective-permute-done.10), channel_id=1, source_target_pairs={{0,8},{8,16},{16,24},{24,32},{32,40},{40,48},{48,56},{56,64},{64,7... | collective-permute-start | bytes 786440 | tf_op jit(solution)/shard_map/ppermute | solution.py:15
  234.3 10.1 %collective-permute-start.13 = (bf16[128,1024]{1,0:T(8,128)(2,1)S(1)}, bf16[128,1024]{1,0:T(8,128)(2,1)S(1)}, u32[]{:S(2)}, u32[]{:S(2)}) collective-permute-start(bf16[128,1024]{1,0:T(8,128)(2,1)S(1)} %collective-permute-done.11), channel_id=1, source_target_pairs={{0,120},{8,0},{16,8},{24,16},{32,24},{40,32},{48,40},{56,48},{64,5... | collective-permute-start | bytes 786440 | tf_op jit(solution)/shard_map/ppermute | solution.py:18
  242.7 9.7 %collective-permute-start.14 = (bf16[128,1024]{1,0:T(8,128)(2,1)S(1)}, bf16[128,1024]{1,0:T(8,128)(2,1)S(1)}, u32[]{:S(2)}, u32[]{:S(2)}) collective-permute-start(bf16[128,1024]{1,0:T(8,128)(2,1)S(1)} %collective-permute-done.12), channel_id=1, source_target_pairs={{0,8},{8,16},{16,24},{24,32},{32,40},{40,48},{48,56},{56,64},{64,7... | collective-permute-start | bytes 786440 | tf_op jit(solution)/shard_map/ppermute | solution.py:15
Sparse Core Ops, SparseCore 0:
  9.7 52.1 all-gather.2
  64.0 51.6 all-gather.4
  146.7 99.1 reduce-scatter.3
